TPU v7x, 32 devices: a whole 2x2x4 slice. The times are simulated.
32 devices in a mesh: ep: 16 (over z, y, x), tp: 2 (over core).
Axes of the slice: x: 2, y: 2, z: 4, core: 2. Of those that a mesh axis runs over, the one named last changes fastest.
Arguments:
- tokens: bfloat16 [512, 2048], P('ep'), may hold values from -6 to 6
- lru_state: float32 [512, 1024], P('ep', 'tp'), may hold values from -6 to 6
- conv_window: bfloat16 [512, 3, 1024], P('ep', None, 'tp'), may hold values from -6 to 6
- gain_mix_in: float32 [2048], replicated, may hold values from 0.1 to 1.9
- gain_mix_out: float32 [2048], replicated, may hold values from 0.1 to 1.9
- gain_ffn_in: float32 [2048], replicated, may hold values from 0.1 to 1.9
- gain_ffn_out: float32 [2048], replicated, may hold values from 0.1 to 1.9
- w_branch: bfloat16 [2048, 1024], P(None, 'tp'), may hold values from -0.125 to 0.125
- w_input: bfloat16 [2048, 1024], P(None, 'tp'), may hold values from -0.125 to 0.125
- conv_taps: bfloat16 [4, 1024], P(None, 'tp'), may hold values from -3 to 3
- gate_a: bfloat16 [8, 128, 128], P('tp'), may hold values from -0.5 to 0.5
- gate_x: bfloat16 [8, 128, 128], P('tp'), may hold values from -0.5 to 0.5
- decay_rate: float32 [1024], P('tp'), may hold values from 0.001 to 0.3
- w_mix_out: bfloat16 [1024, 2048], P('tp'), may hold values from -0.1875 to 0.1875
- routes: int32 [512, 4], P('ep'), may hold values from 0 to 15, all different within a row; in each aligned block of 32 rows (0 to 31, 32 to 63, ...) at most 16 rows name the same one
- route_weight: float32 [512, 4], P('ep'), may hold values from 0.2 to 1.5
- expert_gate: bfloat16 [16, 2048, 512], P('ep', None, 'tp'), may hold values from -0.125 to 0.125
- expert_up: bfloat16 [16, 2048, 512], P('ep', None, 'tp'), may hold values from -0.125 to 0.125
- expert_down: bfloat16 [16, 512, 2048], P('ep', 'tp'), may hold values from -0.25 to 0.25
- shared_gate: bfloat16 [2048, 512], P(None, 'tp'), may hold values from -0.125 to 0.125
- shared_up: bfloat16 [2048, 512], P(None, 'tp'), may hold values from -0.125 to 0.125
- shared_down: bfloat16 [512, 2048], P('tp'), may hold values from -0.25 to 0.25
Outputs:
- layer_out: bfloat16 [512, 2048], P('ep')
- new_state: float32 [512, 1024], P('ep', 'tp')
- new_window: bfloat16 [512, 3, 1024], P('ep', None, 'tp')
Inputs may be any that keep to these rules, and one draw needn't show every extreme that they name: `routes`: each row names 4 different experts. Within the rows of one device (aligned blocks of 32 rows) no expert is named by more than 16 entries, a bound that some block reaches.
All inputs are finite; a program needn't handle non-finite values.
Results may differ from a plain program's by a relative error of at most 0.014.
Values may be sent and summed in bfloat16 or wider, within the bound.
A program may use at most 64 MiB of HBM per device.

v0:
```python
import jax
import jax.numpy as jnp
from jax import lax
from jax.sharding import PartitionSpec as P


def rms_norm(value, gain):
    return value * lax.rsqrt(jnp.mean(value * value, axis=-1, keepdims=True) + 1e-06) * gain


def rounded_term(value):
    return lax.optimization_barrier(value.astype(jnp.bfloat16)).astype(jnp.float32)


def on_device(
    tokens,
    lru_state,
    conv_window,
    gain_mix_in,
    gain_mix_out,
    gain_ffn_in,
    gain_ffn_out,
    w_branch,
    w_input,
    conv_taps,
    gate_a,
    gate_x,
    decay_rate,
    w_mix_out,
    routes,
    route_weight,
    expert_gate,
    expert_up,
    expert_down,
    shared_gate,
    shared_up,
    shared_down,
):
    resid = tokens.astype(jnp.float32)
    normed = rms_norm(resid, gain_mix_in).astype(jnp.bfloat16)
    branch = jnp.dot(normed, w_branch, preferred_element_type=jnp.float32)
    inflow = jnp.dot(normed, w_input, preferred_element_type=jnp.float32).astype(jnp.bfloat16)
    window = jnp.concatenate([conv_window, inflow[:, None, :]], axis=1)
    new_window = window[:, 1:]
    conv = jnp.sum(window.astype(jnp.float32) * conv_taps.astype(jnp.float32)[None], axis=1)
    count, local_ch = conv.shape
    groups, group_dim = (gate_a.shape[0], gate_a.shape[1])
    grouped = conv.astype(jnp.bfloat16).reshape(count, groups, group_dim)
    recur_gate = jax.nn.sigmoid(
        jnp.einsum("sbi,bij->sbj", grouped, gate_a, preferred_element_type=jnp.float32).reshape(
            count, local_ch
        )
    )
    input_gate = jax.nn.sigmoid(
        jnp.einsum("sbi,bij->sbj", grouped, gate_x, preferred_element_type=jnp.float32).reshape(
            count, local_ch
        )
    )
    log_decay = -8.0 * recur_gate * decay_rate[None]
    new_state = (
        jnp.exp(log_decay) * lru_state + jnp.sqrt(-jnp.expm1(2.0 * log_decay)) * conv * input_gate
    )
    gated = (new_state * jax.nn.gelu(branch)).astype(jnp.bfloat16)
    mix_term = rounded_term(jnp.dot(gated, w_mix_out, preferred_element_type=jnp.float32))
    mixed = lax.psum(mix_term.astype(jnp.bfloat16), "tp").astype(jnp.float32)
    middle = (resid + rms_norm(mixed, gain_mix_out)).astype(jnp.bfloat16)
    ffn_in = rms_norm(middle.astype(jnp.float32), gain_ffn_in).astype(jnp.bfloat16)
    width = ffn_in.shape[1]
    top = routes.shape[1]
    local_exp = expert_gate.shape[0]
    experts = local_exp * lax.axis_size("ep")
    capacity = max(2, 2 * count * top // experts)
    flat = routes.reshape(count * top)
    onehot = (flat[:, None] == jnp.arange(experts, dtype=jnp.int32)[None, :]).astype(jnp.int32)
    rank = jnp.sum(onehot * (jnp.cumsum(onehot, axis=0) - 1), axis=-1)
    dest = flat * capacity + rank
    slot_ids = jnp.arange(experts * capacity, dtype=jnp.int32)
    placed = jnp.any(dest.reshape(count, top)[None, :, :] == slot_ids[:, None, None], axis=-1)
    outbound = jnp.dot(placed.astype(jnp.bfloat16), ffn_in, preferred_element_type=jnp.float32)
    outbound = outbound.astype(jnp.bfloat16).reshape(experts, capacity, width)
    shared_hidden = (
        jax.nn.silu(jnp.dot(ffn_in, shared_gate, preferred_element_type=jnp.float32))
        * jnp.dot(ffn_in, shared_up, preferred_element_type=jnp.float32)
    ).astype(jnp.bfloat16)
    shared = lax.psum(
        rounded_term(
            jnp.dot(shared_hidden, shared_down, preferred_element_type=jnp.float32)
        ).astype(jnp.bfloat16),
        "tp",
    ).astype(jnp.float32)
    share = width // lax.axis_size("tp")
    own = lax.dynamic_slice_in_dim(outbound, lax.axis_index("tp") * share, share, 2)
    arrived = lax.all_to_all(own, "ep", split_axis=0, concat_axis=1, tiled=True)
    rows = lax.all_gather(arrived, "tp", axis=2, tiled=True)
    hidden = (
        jax.nn.silu(
            jnp.einsum("erd,edf->erf", rows, expert_gate, preferred_element_type=jnp.float32)
        )
        * jnp.einsum("erd,edf->erf", rows, expert_up, preferred_element_type=jnp.float32)
    ).astype(jnp.bfloat16)
    summed = lax.psum_scatter(
        rounded_term(
            jnp.einsum("erf,efd->erd", hidden, expert_down, preferred_element_type=jnp.float32)
        ).astype(jnp.bfloat16),
        "tp",
        scatter_dimension=2,
        tiled=True,
    )
    back = lax.all_to_all(summed, "ep", split_axis=1, concat_axis=0, tiled=True)
    flat_out = back.reshape(experts * capacity, share)
    picked = flat_out[dest].reshape(count, top, flat_out.shape[1])
    routed_share = jnp.sum(picked.astype(jnp.float32) * route_weight[:, :, None], axis=1).astype(
        jnp.bfloat16
    )
    routed = lax.all_gather(routed_share, "tp", axis=1, tiled=True)
    total = routed.astype(jnp.float32) + shared
    layer_out = (middle.astype(jnp.float32) + rms_norm(total, gain_ffn_out)).astype(jnp.bfloat16)
    return (layer_out, new_state, new_window)


def solution(mesh):
    placed = (
        P("ep", None),
        P("ep", "tp"),
        P("ep", None, "tp"),
        P(),
        P(),
        P(),
        P(),
        P(None, "tp"),
        P(None, "tp"),
        P(None, "tp"),
        P("tp", None, None),
        P("tp", None, None),
        P("tp"),
        P("tp", None),
        P("ep", None),
        P("ep", None),
        P("ep", None, "tp"),
        P("ep", None, "tp"),
        P("ep", "tp", None),
        P(None, "tp"),
        P(None, "tp"),
        P("tp", None),
    )
    return jax.shard_map(
        on_device,
        mesh=mesh,
        in_specs=placed,
        out_specs=(P("ep", None), P("ep", "tp"), P("ep", None, "tp")),
        check_vma=False,
    )
```

profile of v0, /device:TPU:0, one launch (start us, length us, event | category | flops | bytes accessed | tf_op | source)
XLA Modules:
  0.0 134.1 jit_solution(11292914418998984690)
XLA Ops:
  7.3 1.2 fusion.24
  9.2 2.2 %fusion.10 = bf16[32,1,512]{2,0,1:T(8,128)(2,1)S(1)} fusion(bf16[2048,512]{1,0:T(8,128)(2,1)} %param.30, bf16[32,2048]{1,0:T(8,128)(2,1)} %param.22, f32[2048]{0:T(1024)} %param.25, f32[32]{0:T(128)S(1)} %add_rsqrt_fusion.3), kind=kOutput, calls=%fused_computation.19 | convolution fusion | flops 67387392 | bytes 2269312 | tf_op jit(solution)/shard_map/dot_general | solution.py:42
  12.0 3.2 %convolution_convert_fusion.3 = bf16[32,2048]{1,0:T(8,128)(2,1)} fusion(bf16[512,2048]{1,0:T(8,128)(2,1)S(1)} %copy-done, f32[32,512]{1,0:T(8,128)S(1)} %fusion.49, bf16[2048,512]{1,0:T(8,128)(2,1)} %param.29, bf16[32,2048]{1,0:T(8,128)(2,1)S(1)} %copy-done.2, f32[2048]{0:T(1024)S(1)} %copy-done.10, f32[32]{0:T(128)S(1)} %add_rsqrt_fusion.3), kind=kOutput, calls=%fused_computation.5 | convolution fusion | flops 134709248 | bytes 4530304 | tf_op jit(solution)/shard_map/dot_general | solution.py:64
  16.9 19.2 %all-reduce.3.cloned.1.call-done = bf16[32,2048]{1,0:T(8,128)(2,1)} async-done(((bf16[32,2048]{1,0:T(8,128)(2,1)}), bf16[32,2048]{1,0:T(8,128)(2,1)}) %all-reduce.3.cloned.1.call-update) | async-done | bytes 131088 | tf_op jit(solution)/shard_map/psum | solution.py:65
  36.1 1.0 fusion.22
  37.1 1.1 fusion.28
  38.9 22.2 %all_to_all.21 = bf16[16,16,1024]{2,1,0:T(8,128)(2,1)} all-to-all(bf16[16,16,1024]{2,1,0:T(8,128)(2,1)S(1)} %constant_dynamic-slice_fusion), channel_id=1, replica_groups=mesh['ep'=16,'tp'=2] {'ep'}, dimensions={0} | all-to-all | bytes 1048576 | tf_op jit(solution)/shard_map/all_to_all | solution.py:93
  61.1 7.5 %all-gather.2.cloned.1.call-done = bf16[1,256,2048]{2,1,0:T(8,128)(2,1)} async-done(((bf16[1,256,1024]{2,1,0:T(8,128)(2,1)}), bf16[1,256,2048]{2,1,0:T(8,128)(2,1)}) %all-gather.2.cloned.1.call-update) | async-done | bytes 1048592 | tf_op jit(solution)/shard_map/all_gather | solution.py:94
  68.6 2.1 %fusion.14 = f32[256,256]{1,0:T(8,128)S(1)} fusion(bf16[1,2048,256]{2,1,0:T(8,128)(2,1)} %param.38, bf16[1,256,2048]{2,1,0:T(8,128)(2,1)} %all-gather.2.cloned.1.call-done), kind=kOutput, calls=%fused_computation.24 | convolution fusion | flops 268435456 | bytes 2359296 | tf_op jit(solution)/shard_map/erd,edf->erf/dot_general | solution.py:97
  70.7 3.8 %fusion = bf16[1,256,2048]{2,1,0:T(8,128)(2,1)} fusion(bf16[1,256,2048]{2,1,0:T(8,128)(2,1)} %param.40, bf16[1,2048,256]{2,1,0:T(8,128)(2,1)} %param.39, bf16[1,256,2048]{2,1,0:T(8,128)(2,1)S(1)} %copy-done.1, f32[256,256]{1,0:T(8,128)S(1)} %fusion.14), kind=kOutput, calls=%fused_computation.3 | convolution fusion | flops 537788416 | bytes 4456448 | tf_op jit(solution)/shard_map/erf,efd->erd/dot_general | solution.py:103
  76.2 8.1 %reduce-scatter.2.cloned.1.call-done = bf16[1,256,1024]{2,1,0:T(8,128)(2,1)} async-done(((bf16[1,256,2048]{2,1,0:T(8,128)(2,1)}), bf16[1,256,1024]{2,1,0:T(8,128)(2,1)}) %reduce-scatter.2.cloned.1.call-update) | async-done | bytes 524304 | tf_op jit(solution)/shard_map/reduce_scatter | solution.py:101
  84.3 1.9 %copy.81 = bf16[1,256,1024]{2,0,1:T(2,128)(2,1)S(1)} copy(bf16[1,256,1024]{2,1,0:T(8,128)(2,1)} %reduce-scatter.2.cloned.1.call-done) | data formatting | bytes 1048576 | tf_op jit(solution)/shard_map/reduce_scatter | solution.py:101
  86.7 4.5 %reduce = bf16[256,1024]{1,0:T(8,128)(2,1)} reduce(bf16[256,1,1024]{2,1,0:T(2,128)(2,1)S(1)} %bitcast.73, bf16[]{:T(256)} %broadcast.143), dimensions={1}, to_apply=%bitcast.70.reduce_sub_computation | reduce | bytes 1048578
  91.2 2.2 %reshape.155 = bf16[16,2,8192]{2,1,0:T(2,128)(2,1)} reshape(bf16[256,1024]{1,0:T(8,128)(2,1)} %reduce) | data formatting | bytes 1048576
  93.4 6.8 %all-to-all-start.1 = ((bf16[16,2,8192]{2,1,0:T(2,128)(2,1)}), bf16[16,2,8192]{2,1,0:T(2,128)(2,1)S(1)}, u32[]{:S(2)}, u32[]{:S(2)}) async-start(bf16[16,2,8192]{2,1,0:T(2,128)(2,1)} %reshape.155), calls=%async_computation.2 | async-start | bytes 1048576 | tf_op jit(solution)/shard_map/all_to_all | solution.py:109
  100.9 1.5 %fusion.82 = f32[32,256]{1,0:T(8,128)S(1)} fusion(bf16[2048,256]{1,0:T(8,128)(2,1)} %param.41, bf16[32,2048]{1,0:T(8,128)(2,1)S(1)} %get-tuple-element.4, f32[2048]{0:T(1024)S(1)} %copy-done.8, f32[32]{0:T(128)S(1)} %add_rsqrt_fusion.1), kind=kOutput, calls=%fused_computation.113 | convolution fusion | flops 33816576 | bytes 1220736 | tf_op jit(solution)/shard_map/dot_general | solution.py:82
  102.5 3.0 %convolution_convert_fusion.2 = bf16[32,2048]{1,0:T(8,128)(2,1)} fusion(bf16[256,2048]{1,0:T(8,128)(2,1)} %param.43, bf16[2048,256]{1,0:T(8,128)(2,1)} %param.42, f32[32,256]{1,0:T(8,128)S(1)} %fusion.82, bf16[32,2048]{1,0:T(8,128)(2,1)S(1)} %get-tuple-element.4, f32[2048]{0:T(1024)S(1)} %copy-done.8, f32[32]{0:T(128)S(1)} %add_rsqrt_fusion.1), kind=kOutput, calls=%fused_computation.4 | convolution fusion | flops 67485696 | bytes 2400384 | tf_op jit(solution)/shard_map/dot_general | solution.py:87
  105.5 10.2 %all-to-all-done.1 = bf16[16,2,8192]{2,1,0:T(2,128)(2,1)S(1)} async-done(((bf16[16,2,8192]{2,1,0:T(2,128)(2,1)}), bf16[16,2,8192]{2,1,0:T(2,128)(2,1)S(1)}, u32[]{:S(2)}, u32[]{:S(2)}) %all-to-all-start.1) | async-done | bytes 524320 | tf_op jit(solution)/shard_map/all_to_all | solution.py:109
  115.7 1.8 %reshape.156 = bf16[256,1,1024]{2,1,0:T(2,128)(2,1)} reshape(bf16[16,2,8192]{2,1,0:T(2,128)(2,1)S(1)} %all-to-all-done.1) | data formatting | bytes 1048576
  117.4 1.4 %copy.80 = bf16[1,256,1024]{2,1,0:T(8,128)(2,1)S(1)} copy(bf16[1,256,1024]{2,0,1:T(2,128)(2,1)} %bitcast.72) | data formatting | bytes 1048576
  120.3 1.9 %all_gather.7 = bf16[32,2048]{1,0:T(8,128)(2,1)S(1)} all-gather(bf16[32,1024]{1,0:T(8,128)(2,1)S(1)} %multiply_reduce_fusion), channel_id=1, replica_groups=mesh['ep'=16,'tp'=2] {'tp'}, dimensions={1}, use_global_device_ids=true | all-gather | bytes 196608 | tf_op jit(solution)/shard_map/all_gather | solution.py:115
  122.2 2.7 %all-reduce.5.cloned.1.call-done = bf16[32,2048]{1,0:T(8,128)(2,1)} async-done(((bf16[32,2048]{1,0:T(8,128)(2,1)}), bf16[32,2048]{1,0:T(8,128)(2,1)}) %all-reduce.5.cloned.1.call-update) | async-done | bytes 131088 | tf_op jit(solution)/shard_map/psum | solution.py:85
  124.8 1.1 multiply_reduce_fusion.1
  125.9 1.7 %fusion.31 = bf16[32,2048]{1,0:T(8,128)(2,1)} fusion(bf16[32,2048]{1,0:T(8,128)(2,1)S(1)} %get-tuple-element.4, bf16[32,2048]{1,0:T(8,128)(2,1)} %all-reduce.5.cloned.1.call-done, bf16[32,2048]{1,0:T(8,128)(2,1)S(1)} %all_gather.7, f32[2048]{0:T(1024)S(1)} %copy-done.11, f32[32]{0:T(128)S(1)} %add_rsqrt_fusion), kind=kLoop, calls=%fused_computation.47 | loop fusion | flops 524288 | bytes 532608 | tf_op jit(solution)/shard_map/convert_element_type | solution.py:117
  (72 shorter events, 7.7 us)
Async XLA Ops:
  7.2 4.8 %copy-start = (bf16[512,2048]{1,0:T(8,128)(2,1)S(1)}, bf16[512,2048]{1,0:T(8,128)(2,1)}, u32[]{:S(2)}) copy-start(bf16[512,2048]{1,0:T(8,128)(2,1)} %param.35) | copy-start | bytes 6291460
  7.2 4.8 %copy-start.2 = (bf16[32,2048]{1,0:T(8,128)(2,1)S(1)}, bf16[32,2048]{1,0:T(8,128)(2,1)}, u32[]{:S(2)}) copy-start(bf16[32,2048]{1,0:T(8,128)(2,1)} %param.22) | copy-start | bytes 393220
  7.2 4.8 %copy-start.10 = (f32[2048]{0:T(1024)S(1)}, f32[2048]{0:T(1024)}, u32[]{:S(2)}) copy-start(f32[2048]{0:T(1024)} %param.25) | copy-start | bytes 24580
  7.2 4.2 %copy-start.3 = (bf16[32,3,512]{2,0,1:T(8,128)(2,1)S(1)}, bf16[32,3,512]{2,0,1:T(8,128)(2,1)}, u32[]{:S(2)}) copy-start(bf16[32,3,512]{2,0,1:T(8,128)(2,1)} %param.24) | copy-start | bytes 294916
  7.2 4.2 %copy-start.15 = (bf16[4,128,128]{2,1,0:T(8,128)(2,1)S(1)}, bf16[4,128,128]{2,1,0:T(8,128)(2,1)}, u32[]{:S(2)}) copy-start(bf16[4,128,128]{2,1,0:T(8,128)(2,1)} %param.33) | copy-start | bytes 393220
  7.2 4.4 %copy-start.16 = (bf16[4,128,128]{2,1,0:T(8,128)(2,1)S(1)}, bf16[4,128,128]{2,1,0:T(8,128)(2,1)}, u32[]{:S(2)}) copy-start(bf16[4,128,128]{2,1,0:T(8,128)(2,1)} %param.32) | copy-start | bytes 393220
  7.2 4.6 %copy-start.14 = (f32[512]{0:T(512)S(1)}, f32[512]{0:T(512)}, u32[]{:S(2)}) copy-start(f32[512]{0:T(512)} %param.34) | copy-start | bytes 6148
  7.2 4.6 %copy-start.9 = (f32[32,512]{1,0:T(8,128)S(1)}, f32[32,512]{1,0:T(8,128)}, u32[]{:S(2)}) copy-start(f32[32,512]{1,0:T(8,128)} %param.23) | copy-start | bytes 196612
  7.3 28.8 %all-reduce.3.cloned.1.call-start = ((), (), s32[]{:S(2)}) async-start(), calls=%async_computation.3 | async-start | bytes 262144 | tf_op jit(solution)/shard_map/psum | solution.py:65
  11.4 3.8 %copy-start.5 = (bf16[32,1,512]{2,0,1:T(8,128)(2,1)}, bf16[32,1,512]{2,0,1:T(8,128)(2,1)S(1)}, u32[]{:S(2)}) copy-start(bf16[32,1,512]{2,0,1:T(8,128)(2,1)S(1)} %fusion.10) | copy-start | bytes 98308
  12.0 3.3 %copy-start.7 = (f32[32,512]{1,0:T(8,128)}, f32[32,512]{1,0:T(8,128)S(1)}, u32[]{:S(2)}) copy-start(f32[32,512]{1,0:T(8,128)S(1)} %fusion.49) | copy-start | bytes 196612
  12.0 3.4 %copy-start.13 = (s32[32,4]{0,1:T(4,128)S(1)}, s32[32,4]{0,1:T(4,128)}, u32[]{:S(2)}) copy-start(s32[32,4]{0,1:T(4,128)} %param.36) | copy-start | bytes 1540
  12.0 25.1 %copy-start.12 = (f32[2048]{0:T(1024)S(1)}, f32[2048]{0:T(1024)}, u32[]{:S(2)}) copy-start(f32[2048]{0:T(1024)} %param.26) | copy-start | bytes 24580
  12.0 26.3 %copy-start.8 = (f32[2048]{0:T(1024)S(1)}, f32[2048]{0:T(1024)}, u32[]{:S(2)}) copy-start(f32[2048]{0:T(1024)} %param.27) | copy-start | bytes 24580
  15.3 53.4 %all-gather.2.cloned.1.call-start = ((), (), s32[]{:S(2)}) async-start(), calls=%async_computation.4 | async-start | bytes 1572864 | tf_op jit(solution)/shard_map/all_gather | solution.py:94
  61.1 23.2 %reduce-scatter.2.cloned.1.call-start = ((), (), s32[]{:S(2)}) async-start(), calls=%async_computation.5 | async-start | bytes 1572864 | tf_op jit(solution)/shard_map/reduce_scatter | solution.py:101
  68.6 2.1 %copy-start.1 = (bf16[1,256,2048]{2,1,0:T(8,128)(2,1)S(1)}, bf16[1,256,2048]{2,1,0:T(8,128)(2,1)}, u32[]{:S(2)}) copy-start(bf16[1,256,2048]{2,1,0:T(8,128)(2,1)} %all-gather.2.cloned.1.call-done) | copy-start | bytes 3145732
  86.1 14.1 %copy-start.4 = (bf16[32,3,512]{2,0,1:T(8,128)(2,1)S(1)}, bf16[32,3,512]{2,0,1:T(8,128)(2,1)}, u32[]{:S(2)}) copy-start(bf16[32,3,512]{2,0,1:T(8,128)(2,1)} %param.24) | copy-start | bytes 294916
  86.2 14.1 %copy-start.6 = (bf16[32,1,512]{2,0,1:T(8,128)(2,1)S(1)}, bf16[32,1,512]{2,0,1:T(8,128)(2,1)}, u32[]{:S(2)}) copy-start(bf16[32,1,512]{2,0,1:T(8,128)(2,1)} %copy-done.5) | copy-start | bytes 98308
  93.4 22.3 %all-to-all-start.1 = ((bf16[16,2,8192]{2,1,0:T(2,128)(2,1)}), bf16[16,2,8192]{2,1,0:T(2,128)(2,1)S(1)}, u32[]{:S(2)}, u32[]{:S(2)}) async-start(bf16[16,2,8192]{2,1,0:T(2,128)(2,1)} %reshape.155), calls=%async_computation.2 | async-start | bytes 1048576 | tf_op jit(solution)/shard_map/all_to_all | solution.py:109
  100.2 24.7 %all-reduce.5.cloned.1.call-start = ((), (), s32[]{:S(2)}) async-start(), calls=%async_computation.6 | async-start | bytes 262144 | tf_op jit(solution)/shard_map/psum | solution.py:85
  118.8 7.1 %copy-start.11 = (f32[2048]{0:T(1024)S(1)}, f32[2048]{0:T(1024)}, u32[]{:S(2)}) copy-start(f32[2048]{0:T(1024)} %param.28) | copy-start | bytes 24580
Sparse Core Ops, SparseCore 0:
  15.4 20.6 all-reduce.2
  61.2 7.3 all-gather.1
  74.7 9.5 reduce-scatter.1
  105.6 19.1 all-reduce.4
where the time goes:
time: 135 us; the launch traced here: 134 us
  waiting for transfers between devices  47.7 us (35%)
  blocking collectives  24.1 us (18%)
  matrix products  16.7 us (12%)
  between operations  14.2 us (11%)
  other arithmetic  13.6 us (10%)
  local copies, waits for them, and re-layouts  10.9 us (8%)
  starting transfers between devices  6.93 us (5%)
    all_to_all x1, blocking collectives, on_device(): arrived = lax.all_to_all(own, 'ep', split_axis=0, concat_axis=1, tiled=True)  22.2 us
    psum x1, waiting for transfers between devices, on_device(): mixed = lax.psum(mix_term.astype(jnp.bfloat16), 'tp').astype(jnp.float32)  19.2 us
    all_to_all x1, waiting for transfers between devices, on_device(): back = lax.all_to_all(summed, 'ep', split_axis=1, concat_axis=0, tiled=True)  10.2 us
    reduce_scatter x1, waiting for transfers between devices, on_device(): lax.psum_scatter(rounded_term(jnp.einsum('erf,efd->erd', hidden, expert_d...  8.14 us
    all_gather x1, waiting for transfers between devices, on_device(): rows = lax.all_gather(arrived, 'tp', axis=2, tiled=True)  7.49 us
    unnamed x40, local copies, waits for them, and re-layouts  6.86 us
    all_to_all x1, starting transfers between devices, on_device(): back = lax.all_to_all(summed, 'ep', split_axis=1, concat_axis=0, tiled=True)  6.77 us
    unnamed x1, other arithmetic  4.5 us
  transfers between devices with their start and end apart: 5, of which 5 were waited for; matrix products, arithmetic and copies ran while one was open for 10% of the time, Pallas kernels for 0%

commit v1 on v0

--- a/solution.py
+++ b/solution.py
@@ -62,7 +62,8 @@
     )
     gated = (new_state * jax.nn.gelu(branch)).astype(jnp.bfloat16)
     mix_term = rounded_term(jnp.dot(gated, w_mix_out, preferred_element_type=jnp.float32))
-    mixed = lax.psum(mix_term.astype(jnp.bfloat16), "tp").astype(jnp.float32)
+    follow_quotas_up = lambda local, device_axis: lax.all_gather(local, device_axis).sum(axis=0)
+    mixed = follow_quotas_up(mix_term.astype(jnp.bfloat16), "tp").astype(jnp.float32)
     middle = (resid + rms_norm(mixed, gain_mix_out)).astype(jnp.bfloat16)
     ffn_in = rms_norm(middle.astype(jnp.float32), gain_ffn_in).astype(jnp.bfloat16)
     width = ffn_in.shape[1]

time: 135 us -> 116 us (0.86)
  waiting for transfers between devices: 47.7 us -> 29.1 us
  blocking collectives: 24.1 us -> 27.5 us
  other arithmetic: 13.6 us -> 11.9 us
    psum x1 -> x0, waiting for transfers between devices: 19.2 us -> none  [on_device(): mixed = lax.psum(mix_term.astype(jnp.bfloat16), 'tp').astype(jnp.float32)]
    all_gather x0 -> x1, blocking collectives: none -> 2.12 us  [on_device(): lax.all_gather(local, device_axis).sum(axis=0)]
    reduce_sum x4, other arithmetic: 4.42 us -> 2.62 us  [rms_norm(): jnp.mean(value * value, axis=-1, keepdims=True) + 1e-06]
    reduce_scatter x1, waiting for transfers between devices: 8.14 us -> 9.7 us  [on_device(): lax.psum_scatter(rounded_term(jnp.einsum('erf,efd->erd', hidden, expert_d...]
    unnamed x40 -> x44, local copies, waits for them, and re-layouts: 6.86 us -> 6.37 us
  transfers between devices with their start and end apart: 5 -> 4, of which waited for: 5 -> 4; matrix products, arithmetic and copies ran while one was open for 10% -> 9% of each run, Pallas kernels for 0% -> 0%
where the time goes in v1:
time: 116 us; the launch traced here: 115 us
  waiting for transfers between devices  29.1 us (25%)
  blocking collectives  27.5 us (24%)
  matrix products  16 us (14%)
  between operations  14.2 us (12%)
  other arithmetic  11.9 us (10%)
  local copies, waits for them, and re-layouts  9.69 us (8%)
  starting transfers between devices  6.92 us (6%)
    all_to_all x1, blocking collectives, on_device(): arrived = lax.all_to_all(own, 'ep', split_axis=0, concat_axis=1, tiled=True)  23.5 us
    all_to_all x1, waiting for transfers between devices, on_device(): back = lax.all_to_all(summed, 'ep', split_axis=1, concat_axis=0, tiled=True)  9.93 us
    reduce_scatter x1, waiting for transfers between devices, on_device(): lax.psum_scatter(rounded_term(jnp.einsum('erf,efd->erd', hidden, expert_d...  9.7 us
    all_gather x1, waiting for transfers between devices, on_device(): rows = lax.all_gather(arrived, 'tp', axis=2, tiled=True)  7.46 us
    all_to_all x1, starting transfers between devices, on_device(): back = lax.all_to_all(summed, 'ep', split_axis=1, concat_axis=0, tiled=True)  6.79 us
    unnamed x44, local copies, waits for them, and re-layouts  6.37 us
    unnamed x1, other arithmetic  4.5 us
    dot_general x1, matrix products, on_device(): jnp.einsum('erf,efd->erd', hidden, expert_down, preferred_element_type=jn...  3.82 us
  transfers between devices with their start and end apart: 4, of which 4 were waited for; matrix products, arithmetic and copies ran while one was open for 9% of the time, Pallas kernels for 0%

profile of v1, /device:TPU:0, one launch (start us, length us, event | category | flops | bytes accessed | tf_op | source)
XLA Modules:
  0.0 115.3 jit_solution(774264285441566568)
XLA Ops:
  7.3 1.2 %fusion.24 = f32[32]{0:T(128)S(1)} fusion(bf16[32,2048]{1,0:T(8,128)(2,1)} %param.22), kind=kLoop, calls=%fused_computation.40 | loop fusion | flops 196576 | bytes 131200 | tf_op jit(solution)/shard_map/reduce_sum | solution.py:8
  8.5 0.7 convert_element_type.94
  9.2 2.2 %fusion.10 = bf16[32,1,512]{2,0,1:T(8,128)(2,1)S(1)} fusion(bf16[2048,512]{1,0:T(8,128)(2,1)} %param.30, bf16[32,2048]{1,0:T(8,128)(2,1)} %param.22, f32[2048]{0:T(1024)} %param.25, f32[32]{0:T(128)S(1)} %add_rsqrt_fusion.3), kind=kOutput, calls=%fused_computation.19 | convolution fusion | flops 67387392 | bytes 2269312 | tf_op jit(solution)/shard_map/dot_general | solution.py:42
  12.2 2.6 %convolution_convert_fusion.3 = bf16[32,2048]{1,0:T(8,128)(2,1)S(1)} fusion(bf16[512,2048]{1,0:T(8,128)(2,1)S(1)} %copy-done, f32[32,512]{1,0:T(8,128)S(1)} %fusion.49, bf16[2048,512]{1,0:T(8,128)(2,1)} %param.29, bf16[32,2048]{1,0:T(8,128)(2,1)S(1)} %copy-done.2, f32[2048]{0:T(1024)S(1)} %copy-done.11, f32[32]{0:T(128)S(1)} %add_rsqrt_fusion.3), kind=kOutput, calls=%fused_computation.5 | convolution fusion | flops 134709248 | bytes 4530304 | tf_op jit(solution)/shard_map/dot_general | solution.py:64
  14.8 2.1 %all-gather = bf16[64,2048]{1,0:T(8,128)(2,1)S(1)} all-gather(bf16[32,2048]{1,0:T(8,128)(2,1)S(1)} %convolution_convert_fusion.3), channel_id=2, replica_groups=mesh['ep'=16,'tp'=2] {'tp'}, dimensions={0}, use_global_device_ids=true | all-gather | bytes 393216 | tf_op jit(solution)/shard_map/all_gather | solution.py:65
  19.5 23.5 %all_to_all.21 = bf16[16,16,1024]{2,1,0:T(8,128)(2,1)} all-to-all(bf16[16,16,1024]{2,1,0:T(8,128)(2,1)S(1)} %constant_dynamic-slice_fusion), channel_id=1, replica_groups=mesh['ep'=16,'tp'=2] {'ep'}, dimensions={0} | all-to-all | bytes 1048576 | tf_op jit(solution)/shard_map/all_to_all | solution.py:94
  43.1 7.5 %all-gather.3.cloned.1.call-done = bf16[1,256,2048]{2,1,0:T(8,128)(2,1)} async-done(((bf16[1,256,1024]{2,1,0:T(8,128)(2,1)}), bf16[1,256,2048]{2,1,0:T(8,128)(2,1)}) %all-gather.3.cloned.1.call-update) | async-done | bytes 1048592 | tf_op jit(solution)/shard_map/all_gather | solution.py:95
  50.5 2.1 %fusion.14 = f32[256,256]{1,0:T(8,128)S(1)} fusion(bf16[1,2048,256]{2,1,0:T(8,128)(2,1)} %param.38, bf16[1,256,2048]{2,1,0:T(8,128)(2,1)} %all-gather.3.cloned.1.call-done), kind=kOutput, calls=%fused_computation.24 | convolution fusion | flops 268435456 | bytes 2359296 | tf_op jit(solution)/shard_map/erd,edf->erf/dot_general | solution.py:98
  52.6 3.8 %fusion = bf16[1,256,2048]{2,1,0:T(8,128)(2,1)} fusion(bf16[1,256,2048]{2,1,0:T(8,128)(2,1)} %param.40, bf16[1,2048,256]{2,1,0:T(8,128)(2,1)} %param.39, bf16[1,256,2048]{2,1,0:T(8,128)(2,1)S(1)} %copy-done.1, f32[256,256]{1,0:T(8,128)S(1)} %fusion.14), kind=kOutput, calls=%fused_computation.3 | convolution fusion | flops 537788416 | bytes 4456448 | tf_op jit(solution)/shard_map/erf,efd->erd/dot_general | solution.py:104
  56.5 9.7 %reduce-scatter.2.cloned.1.call-done = bf16[1,256,1024]{2,1,0:T(8,128)(2,1)} async-done(((bf16[1,256,2048]{2,1,0:T(8,128)(2,1)}), bf16[1,256,1024]{2,1,0:T(8,128)(2,1)}) %reduce-scatter.2.cloned.1.call-update) | async-done | bytes 524304 | tf_op jit(solution)/shard_map/reduce_scatter | solution.py:102
  66.2 1.9 %copy.81 = bf16[1,256,1024]{2,0,1:T(2,128)(2,1)S(1)} copy(bf16[1,256,1024]{2,1,0:T(8,128)(2,1)} %reduce-scatter.2.cloned.1.call-done) | data formatting | bytes 1048576 | tf_op jit(solution)/shard_map/reduce_scatter | solution.py:102
  68.5 4.5 %reduce.1 = bf16[256,1024]{1,0:T(8,128)(2,1)} reduce(bf16[256,1,1024]{2,1,0:T(2,128)(2,1)S(1)} %bitcast.74, bf16[]{:T(256)} %broadcast.143), dimensions={1}, to_apply=%bitcast.71.reduce_sub_computation | reduce | bytes 1048578
  73.0 2.2 %reshape.156 = bf16[16,2,8192]{2,1,0:T(2,128)(2,1)} reshape(bf16[256,1024]{1,0:T(8,128)(2,1)} %reduce.1) | data formatting | bytes 1048576
  75.2 6.8 %all-to-all-start.1 = ((bf16[16,2,8192]{2,1,0:T(2,128)(2,1)}), bf16[16,2,8192]{2,1,0:T(2,128)(2,1)S(1)}, u32[]{:S(2)}, u32[]{:S(2)}) async-start(bf16[16,2,8192]{2,1,0:T(2,128)(2,1)} %reshape.156), calls=%async_computation.2 | async-start | bytes 1048576 | tf_op jit(solution)/shard_map/all_to_all | solution.py:110
  82.1 1.5 %fusion.82 = f32[32,256]{1,0:T(8,128)S(1)} fusion(bf16[2048,256]{1,0:T(8,128)(2,1)} %param.41, bf16[32,2048]{1,0:T(8,128)(2,1)S(1)} %get-tuple-element.4, f32[2048]{0:T(1024)S(1)} %copy-done.8, f32[32]{0:T(128)S(1)} %add_rsqrt_fusion.1), kind=kOutput, calls=%fused_computation.113 | convolution fusion | flops 33816576 | bytes 1220736 | tf_op jit(solution)/shard_map/dot_general | solution.py:83
  83.7 3.0 %convolution_convert_fusion.2 = bf16[32,2048]{1,0:T(8,128)(2,1)} fusion(bf16[256,2048]{1,0:T(8,128)(2,1)} %param.43, bf16[2048,256]{1,0:T(8,128)(2,1)} %param.42, f32[32,256]{1,0:T(8,128)S(1)} %fusion.82, bf16[32,2048]{1,0:T(8,128)(2,1)S(1)} %get-tuple-element.4, f32[2048]{0:T(1024)S(1)} %copy-done.8, f32[32]{0:T(128)S(1)} %add_rsqrt_fusion.1), kind=kOutput, calls=%fused_computation.4 | convolution fusion | flops 67485696 | bytes 2400384 | tf_op jit(solution)/shard_map/dot_general | solution.py:88
  87.6 9.9 %all-to-all-done.1 = bf16[16,2,8192]{2,1,0:T(2,128)(2,1)S(1)} async-done(((bf16[16,2,8192]{2,1,0:T(2,128)(2,1)}), bf16[16,2,8192]{2,1,0:T(2,128)(2,1)S(1)}, u32[]{:S(2)}, u32[]{:S(2)}) %all-to-all-start.1) | async-done | bytes 524320 | tf_op jit(solution)/shard_map/all_to_all | solution.py:110
  97.5 1.8 %reshape.157 = bf16[256,1,1024]{2,1,0:T(2,128)(2,1)} reshape(bf16[16,2,8192]{2,1,0:T(2,128)(2,1)S(1)} %all-to-all-done.1) | data formatting | bytes 1048576
  99.3 1.4 %copy.80 = bf16[1,256,1024]{2,1,0:T(8,128)(2,1)S(1)} copy(bf16[1,256,1024]{2,0,1:T(2,128)(2,1)} %bitcast.73) | data formatting | bytes 1048576
  100.7 0.9 gather_fusion
  102.1 1.9 %all_gather.15 = bf16[32,2048]{1,0:T(8,128)(2,1)S(1)} all-gather(bf16[32,1024]{1,0:T(8,128)(2,1)S(1)} %multiply_reduce_fusion), channel_id=1, replica_groups=mesh['ep'=16,'tp'=2] {'tp'}, dimensions={1}, use_global_device_ids=true | all-gather | bytes 196608 | tf_op jit(solution)/shard_map/all_gather | solution.py:116
  104.0 2.0 %all-reduce.2.cloned.1.call-done = bf16[32,2048]{1,0:T(8,128)(2,1)} async-done(((bf16[32,2048]{1,0:T(8,128)(2,1)}), bf16[32,2048]{1,0:T(8,128)(2,1)}) %all-reduce.2.cloned.1.call-update) | async-done | bytes 131088 | tf_op jit(solution)/shard_map/psum | solution.py:86
  106.1 1.1 multiply_reduce_fusion.1
  107.1 1.7 %fusion.31 = bf16[32,2048]{1,0:T(8,128)(2,1)} fusion(bf16[32,2048]{1,0:T(8,128)(2,1)S(1)} %get-tuple-element.4, bf16[32,2048]{1,0:T(8,128)(2,1)} %all-reduce.2.cloned.1.call-done, bf16[32,2048]{1,0:T(8,128)(2,1)S(1)} %all_gather.15, f32[2048]{0:T(1024)S(1)} %copy-done.12, f32[32]{0:T(128)S(1)} %add_rsqrt_fusion), kind=kLoop, calls=%fused_computation.47 | loop fusion | flops 524288 | bytes 532608 | tf_op jit(solution)/shard_map/convert_element_type | solution.py:118
  (75 shorter events, 5.3 us)
Async XLA Ops:
  7.2 4.9 %copy-start = (bf16[512,2048]{1,0:T(8,128)(2,1)S(1)}, bf16[512,2048]{1,0:T(8,128)(2,1)}, u32[]{:S(2)}) copy-start(bf16[512,2048]{1,0:T(8,128)(2,1)} %param.35) | copy-start | bytes 6291460
  7.2 4.9 %copy-start.2 = (bf16[32,2048]{1,0:T(8,128)(2,1)S(1)}, bf16[32,2048]{1,0:T(8,128)(2,1)}, u32[]{:S(2)}) copy-start(bf16[32,2048]{1,0:T(8,128)(2,1)} %param.22) | copy-start | bytes 393220
  7.2 4.9 %copy-start.11 = (f32[2048]{0:T(1024)S(1)}, f32[2048]{0:T(1024)}, u32[]{:S(2)}) copy-start(f32[2048]{0:T(1024)} %param.25) | copy-start | bytes 24580
  7.2 4.2 %copy-start.3 = (bf16[32,3,512]{2,0,1:T(8,128)(2,1)S(1)}, bf16[32,3,512]{2,0,1:T(8,128)(2,1)}, u32[]{:S(2)}) copy-start(bf16[32,3,512]{2,0,1:T(8,128)(2,1)} %param.24) | copy-start | bytes 294916
  7.2 4.2 %copy-start.17 = (bf16[4,128,128]{2,1,0:T(8,128)(2,1)S(1)}, bf16[4,128,128]{2,1,0:T(8,128)(2,1)}, u32[]{:S(2)}) copy-start(bf16[4,128,128]{2,1,0:T(8,128)(2,1)} %param.33) | copy-start | bytes 393220
  7.2 4.4 %copy-start.18 = (bf16[4,128,128]{2,1,0:T(8,128)(2,1)S(1)}, bf16[4,128,128]{2,1,0:T(8,128)(2,1)}, u32[]{:S(2)}) copy-start(bf16[4,128,128]{2,1,0:T(8,128)(2,1)} %param.32) | copy-start | bytes 393220
  7.2 4.6 %copy-start.16 = (f32[512]{0:T(512)S(1)}, f32[512]{0:T(512)}, u32[]{:S(2)}) copy-start(f32[512]{0:T(512)} %param.34) | copy-start | bytes 6148
  7.2 4.8 %copy-start.9 = (f32[32,512]{1,0:T(8,128)S(1)}, f32[32,512]{1,0:T(8,128)}, u32[]{:S(2)}) copy-start(f32[32,512]{1,0:T(8,128)} %param.23) | copy-start | bytes 196612
  7.3 43.3 %all-gather.3.cloned.1.call-start = ((), (), s32[]{:S(2)}) async-start(), calls=%async_computation.3 | async-start | bytes 1572864 | tf_op jit(solution)/shard_map/all_gather | solution.py:95
  11.4 0.6 copy-start.5
  12.1 2.6 %copy-start.7 = (f32[32,512]{1,0:T(8,128)}, f32[32,512]{1,0:T(8,128)S(1)}, u32[]{:S(2)}) copy-start(f32[32,512]{1,0:T(8,128)S(1)} %fusion.49) | copy-start | bytes 196612
  12.1 5.0 %copy-start.13 = (f32[2048]{0:T(1024)S(1)}, f32[2048]{0:T(1024)}, u32[]{:S(2)}) copy-start(f32[2048]{0:T(1024)} %param.26) | copy-start | bytes 24580
  12.2 5.2 %copy-start.14 = (s32[32,4]{0,1:T(4,128)S(1)}, s32[32,4]{0,1:T(4,128)}, u32[]{:S(2)}) copy-start(s32[32,4]{0,1:T(4,128)} %param.36) | copy-start | bytes 1540
  12.2 6.7 %copy-start.8 = (f32[2048]{0:T(1024)S(1)}, f32[2048]{0:T(1024)}, u32[]{:S(2)}) copy-start(f32[2048]{0:T(1024)} %param.27) | copy-start | bytes 24580
  43.0 23.1 %reduce-scatter.2.cloned.1.call-start = ((), (), s32[]{:S(2)}) async-start(), calls=%async_computation.4 | async-start | bytes 1572864 | tf_op jit(solution)/shard_map/reduce_scatter | solution.py:102
  50.5 2.1 %copy-start.1 = (bf16[1,256,2048]{2,1,0:T(8,128)(2,1)S(1)}, bf16[1,256,2048]{2,1,0:T(8,128)(2,1)}, u32[]{:S(2)}) copy-start(bf16[1,256,2048]{2,1,0:T(8,128)(2,1)} %all-gather.3.cloned.1.call-done) | copy-start | bytes 3145732
  75.2 22.3 %all-to-all-start.1 = ((bf16[16,2,8192]{2,1,0:T(2,128)(2,1)}), bf16[16,2,8192]{2,1,0:T(2,128)(2,1)S(1)}, u32[]{:S(2)}, u32[]{:S(2)}) async-start(bf16[16,2,8192]{2,1,0:T(2,128)(2,1)} %reshape.156), calls=%async_computation.2 | async-start | bytes 1048576 | tf_op jit(solution)/shard_map/all_to_all | solution.py:110
  82.0 4.7 %copy-start.10 = (s32[32,4]{1,0:T(8,128)S(1)}, s32[32,4]{1,0:T(8,128)}, u32[]{:S(2)}) copy-start(s32[32,4]{1,0:T(8,128)} %get-tuple-element.5) | copy-start | bytes 1540
  82.0 4.8 %copy-start.15 = (f32[32,4]{0,1:T(4,128)S(1)}, f32[32,4]{0,1:T(4,128)}, u32[]{:S(2)}) copy-start(f32[32,4]{0,1:T(4,128)} %param.37) | copy-start | bytes 1540
  82.1 4.9 %copy-start.4 = (bf16[32,3,512]{2,0,1:T(8,128)(2,1)S(1)}, bf16[32,3,512]{2,0,1:T(8,128)(2,1)}, u32[]{:S(2)}) copy-start(bf16[32,3,512]{2,0,1:T(8,128)(2,1)} %param.24) | copy-start | bytes 294916
  82.1 4.9 %copy-start.6 = (bf16[32,1,512]{2,0,1:T(8,128)(2,1)S(1)}, bf16[32,1,512]{2,0,1:T(8,128)(2,1)}, u32[]{:S(2)}) copy-start(bf16[32,1,512]{2,0,1:T(8,128)(2,1)} %copy-done.5) | copy-start | bytes 98308
  82.1 24.0 %all-reduce.2.cloned.1.call-start = ((), (), s32[]{:S(2)}) async-start(), calls=%async_computation.5 | async-start | bytes 262144 | tf_op jit(solution)/shard_map/psum | solution.py:86
  100.7 6.4 %copy-start.12 = (f32[2048]{0:T(1024)S(1)}, f32[2048]{0:T(1024)}, u32[]{:S(2)}) copy-start(f32[2048]{0:T(1024)} %param.28) | copy-start | bytes 24580
Sparse Core Ops, SparseCore 0:
  43.1 7.3 all-gather.2
  56.6 9.5 reduce-scatter.1
  86.8 19.1 all-reduce.1
